TPU v7x, 32 devices: a whole 2x2x4 slice. The times are simulated.
32 devices in a mesh: fs: 4 (over y, x), tp: 8 (over z, core).
Axes of the slice: x: 2, y: 2, z: 4, core: 2. Of those that a mesh axis runs over, the one named last changes fastest.
Arguments:
- inputs: bfloat16 [1536, 2048], P('fs'), may hold values from -6 to 6
- pre_act: bfloat16 [1536, 8192], P('fs', 'tp'), may hold values from -6 to 6
- cotangent: bfloat16 [1536, 2048], P('fs'), may hold values from -6 to 6
- up_weight: bfloat16 [2048, 8192], P('fs', 'tp'), may hold values from -0.125 to 0.125
- down_weight: bfloat16 [8192, 2048], P('tp', 'fs'), may hold values from -0.0625 to 0.0625
Outputs:
- input_grad: bfloat16 [1536, 2048], P('fs')
- up_grad: float32 [2048, 8192], P('fs', 'tp')
- down_grad: float32 [8192, 2048], P('tp', 'fs')
- up_norms: float32 [2048], P('fs')
- down_norms: float32 [8192], P('tp')
All inputs are finite; a program needn't handle non-finite values.
Results may differ from a plain program's by a relative error of at most 0.0051.
Values may be sent and summed in bfloat16 or wider, within the bound.
A program may use at most 64 MiB of HBM per device.

v0:
```python
import jax
import jax.numpy as jnp
from jax import lax
from jax.sharding import PartitionSpec as P


def contract_last(left, right):
    return lax.dot_general(
        left, right, (((1,), (1,)), ((), ())), preferred_element_type=jnp.float32
    )


def contract_first(left, right):
    return lax.dot_general(
        left, right, (((0,), (0,)), ((), ())), preferred_element_type=jnp.float32
    )


def local(inputs, pre_act, cotangent, up_weight, down_weight):
    active = jnp.maximum(pre_act.astype(jnp.float32), 0.0)
    squared = (active * active).astype(jnp.bfloat16)
    sq_grad = contract_last(cotangent, lax.all_gather(down_weight, "fs", axis=1, tiled=True))
    pre_grad = (2.0 * active * sq_grad).astype(jnp.bfloat16)
    partial_value = contract_last(pre_grad, lax.all_gather(up_weight, "fs", axis=0, tiled=True))
    input_grad = lax.psum(partial_value, "tp").astype(jnp.bfloat16)
    input_cols, cotan_cols = (
        lax.all_to_all(inputs, "fs", split_axis=1, concat_axis=0, tiled=True),
        lax.all_to_all(cotangent, "fs", split_axis=1, concat_axis=0, tiled=True),
    )
    all_pre_grad, all_squared = (
        lax.all_gather(pre_grad, "fs", axis=0, tiled=True),
        lax.all_gather(squared, "fs", axis=0, tiled=True),
    )
    up_grad = contract_first(input_cols, all_pre_grad)
    down_grad = contract_first(all_squared, cotan_cols)
    up_norms = lax.psum(jnp.sum(up_grad * up_grad, axis=1), "tp")
    down_norms = lax.psum(jnp.sum(down_grad * down_grad, axis=1), "fs")
    return (input_grad, up_grad, down_grad, up_norms, down_norms)


def solution(mesh):
    in_specs = (P("fs", None), P("fs", "tp"), P("fs", None), P("fs", "tp"), P("tp", "fs"))
    out_specs = (P("fs", None), P("fs", "tp"), P("tp", "fs"), P("fs"), P("tp"))
    return jax.shard_map(local, mesh=mesh, in_specs=in_specs, out_specs=out_specs, check_vma=False)
```

profile of v0, /device:TPU:0, one launch (start us, length us, event | category | flops | bytes accessed | tf_op | source)
XLA Modules:
  0.0 329.2 jit_solution(1895293256298894493)
XLA Ops:
  7.2 0.7 all-gather.5.cloned.1.call-update
  8.0 0.3 copy-done.2
  8.3 1.1 multiply_convert_fusion
  9.4 0.0 all-gather.7.cloned.1.call-start
  9.5 0.7 all-gather.7.cloned.1.call-update
  10.2 54.8 %all-gather.5.cloned.1.call-done = bf16[1024,2048]{1,0:T(8,128)(2,1)} async-done(((bf16[1024,512]{1,0:T(8,128)(2,1)}), bf16[1024,2048]{1,0:T(8,128)(2,1)}) %all-gather.5.cloned.1.call-update) | async-done | bytes 4194320 | tf_op jit(solution)/shard_map/all_gather | solution.py:22
  65.0 5.2 %multiply_convert_fusion.1 = bf16[384,1024]{1,0:T(8,128)(2,1)} fusion(bf16[384,1024]{1,0:T(8,128)(2,1)} %param.6, bf16[384,2048]{1,0:T(8,128)(2,1)S(1)} %copy-done.1, bf16[1024,2048]{1,0:T(8,128)(2,1)} %all-gather.5.cloned.1.call-done), kind=kOutput, calls=%fused_computation.4 | convolution fusion | flops 1612578816 | bytes 7340032 | tf_op jit(solution)/shard_map/dot_general | solution.py:8
  70.3 1.6 copy.14
  71.8 3.6 %all-to-all-start = ((bf16[384,4,512]{0,2,1:T(8,128)(2,1)}), bf16[384,4,512]{0,2,1:T(8,128)(2,1)S(1)}, u32[]{:S(2)}, u32[]{:S(2)}) async-start(bf16[384,4,512]{0,2,1:T(8,128)(2,1)} %bitcast), calls=%async_computation | async-start | bytes 3145728 | tf_op jit(solution)/shard_map/all_to_all | solution.py:27
  75.5 1.6 copy.16
  77.0 25.8 %all-to-all-done = bf16[384,4,512]{0,2,1:T(8,128)(2,1)S(1)} async-done(((bf16[384,4,512]{0,2,1:T(8,128)(2,1)}), bf16[384,4,512]{0,2,1:T(8,128)(2,1)S(1)}, u32[]{:S(2)}, u32[]{:S(2)}) %all-to-all-start) | async-done | bytes 1572896 | tf_op jit(solution)/shard_map/all_to_all | solution.py:27
  102.9 3.6 %all-to-all-start.1 = ((bf16[384,4,512]{0,2,1:T(8,128)(2,1)}), bf16[384,4,512]{0,2,1:T(8,128)(2,1)S(1)}, u32[]{:S(2)}, u32[]{:S(2)}) async-start(bf16[384,4,512]{0,2,1:T(8,128)(2,1)} %bitcast.4), calls=%async_computation.1 | async-start | bytes 3145728 | tf_op jit(solution)/shard_map/all_to_all | solution.py:28
  106.4 1.6 copy.15
  108.1 34.6 %all-to-all-done.1 = bf16[384,4,512]{0,2,1:T(8,128)(2,1)S(1)} async-done(((bf16[384,4,512]{0,2,1:T(8,128)(2,1)}), bf16[384,4,512]{0,2,1:T(8,128)(2,1)S(1)}, u32[]{:S(2)}, u32[]{:S(2)}) %all-to-all-start.1) | async-done | bytes 1572896 | tf_op jit(solution)/shard_map/all_to_all | solution.py:28
  142.7 1.6 copy.17
  144.3 4.2 %multiply_reduce_fusion = (f32[1024]{0:T(1024)S(1)}, f32[1024,512]{0,1:T(8,128)S(1)}) fusion(bf16[1536,1024]{1,0:T(8,128)(2,1)} %all-gather.11.cloned.1.call-done, bf16[1536,512]{1,0:T(8,128)(2,1)} %bitcast.19), kind=kOutput, calls=%fused_computation | convolution fusion | flops 1611660288 | bytes 6819840 | tf_op jit(solution)/shard_map/dot_general | solution.py:14
  148.5 1.8 copy.19
  150.3 9.8 %psum.23 = f32[1024]{0:T(1024)} all-reduce(f32[1024]{0:T(1024)S(1)} %get-tuple-element.24), channel_id=1, replica_groups=mesh['fs'=4,'tp'=8] {'fs'}, use_global_device_ids=true, to_apply=%region_4.0 | all-reduce | flops 1024 | bytes 8192 | tf_op jit(solution)/shard_map/psum | solution.py:37
  160.1 37.4 %all-gather.7.cloned.1.call-done = bf16[2048,1024]{1,0:T(8,128)(2,1)} async-done(((bf16[512,1024]{1,0:T(8,128)(2,1)}), bf16[2048,1024]{1,0:T(8,128)(2,1)}) %all-gather.7.cloned.1.call-update) | async-done | bytes 4194320 | tf_op jit(solution)/shard_map/all_gather | solution.py:24
  197.5 4.3 %fusion = f32[384,2048]{1,0:T(8,128)S(1)} fusion(bf16[384,1024]{1,0:T(8,128)(2,1)} %multiply_convert_fusion.1, bf16[2048,1024]{1,0:T(8,128)(2,1)} %all-gather.7.cloned.1.call-done), kind=kOutput, calls=%fused_computation.6 | convolution fusion | flops 1610612736 | bytes 8126464 | tf_op jit(solution)/shard_map/dot_general | solution.py:8
  201.7 41.9 %all-gather.9.cloned.1.call-done = bf16[1536,1024]{1,0:T(8,128)(2,1)} async-done(((bf16[384,1024]{1,0:T(8,128)(2,1)}), bf16[1536,1024]{1,0:T(8,128)(2,1)}) %all-gather.9.cloned.1.call-update) | async-done | bytes 3145744 | tf_op jit(solution)/shard_map/all_gather | solution.py:31
  243.6 5.5 %multiply_reduce_fusion.1 = (f32[512]{0:T(512)S(1)}, f32[512,1024]{0,1:T(8,128)}) fusion(bf16[1536,1024]{1,0:T(8,128)(2,1)} %all-gather.9.cloned.1.call-done, bf16[1536,512]{1,0:T(8,128)(2,1)} %bitcast.18), kind=kOutput, calls=%fused_computation.1 | convolution fusion | flops 1611660800 | bytes 6817792 | tf_op jit(solution)/shard_map/dot_general | solution.py:14
  249.1 2.9 copy.18
  252.0 70.7 %all-reduce.2 = (bf16[384,2048]{1,0:T(8,128)(2,1)}, f32[512]{0:T(512)}) all-reduce(f32[384,2048]{1,0:T(8,128)S(1)} %fusion, f32[512]{0:T(512)S(1)} %get-tuple-element.22), channel_id=1, replica_groups=mesh['fs'=4,'tp'=8] {'tp'}, use_global_device_ids=true, to_apply=%region_0.0 | all-reduce | flops 786944 | bytes 4722688 | tf_op jit(solution)/shard_map/psum | solution.py:25
  (11 shorter events, 0.2 us)
Async XLA Ops:
  7.2 1.1 copy-start.2
  7.2 57.8 %all-gather.5.cloned.1.call-start = ((), (), s32[]{:S(2)}) async-start(), calls=%async_computation.2 | async-start | bytes 5242880 | tf_op jit(solution)/shard_map/all_gather | solution.py:22
  7.9 57.1 %copy-start.1 = (bf16[384,2048]{1,0:T(8,128)(2,1)S(1)}, bf16[384,2048]{1,0:T(8,128)(2,1)}, u32[]{:S(2)}) copy-start(bf16[384,2048]{1,0:T(8,128)(2,1)} %param.7) | copy-start | bytes 4718596
  7.9 136.4 %all-gather.11.cloned.1.call-start = ((), (), s32[]{:S(2)}) async-start(), calls=%async_computation.5 | async-start | bytes 3932160 | tf_op jit(solution)/shard_map/all_gather | solution.py:32
  9.4 188.1 %all-gather.7.cloned.1.call-start = ((), (), s32[]{:S(2)}) async-start(), calls=%async_computation.3 | async-start | bytes 5242880 | tf_op jit(solution)/shard_map/all_gather | solution.py:24
  10.1 233.5 %all-gather.9.cloned.1.call-start = ((), (), s32[]{:S(2)}) async-start(), calls=%async_computation.4 | async-start | bytes 3932160 | tf_op jit(solution)/shard_map/all_gather | solution.py:31
  65.0 5.3 %copy-start = (bf16[384,2048]{1,0:T(8,128)(2,1)S(1)}, bf16[384,2048]{1,0:T(8,128)(2,1)}, u32[]{:S(2)}) copy-start(bf16[384,2048]{1,0:T(8,128)(2,1)} %param.5) | copy-start | bytes 4718596
  71.8 31.0 %all-to-all-start = ((bf16[384,4,512]{0,2,1:T(8,128)(2,1)}), bf16[384,4,512]{0,2,1:T(8,128)(2,1)S(1)}, u32[]{:S(2)}, u32[]{:S(2)}) async-start(bf16[384,4,512]{0,2,1:T(8,128)(2,1)} %bitcast), calls=%async_computation | async-start | bytes 3145728 | tf_op jit(solution)/shard_map/all_to_all | solution.py:27
  102.9 39.8 %all-to-all-start.1 = ((bf16[384,4,512]{0,2,1:T(8,128)(2,1)}), bf16[384,4,512]{0,2,1:T(8,128)(2,1)S(1)}, u32[]{:S(2)}, u32[]{:S(2)}) async-start(bf16[384,4,512]{0,2,1:T(8,128)(2,1)} %bitcast.4), calls=%async_computation.1 | async-start | bytes 3145728 | tf_op jit(solution)/shard_map/all_to_all | solution.py:28
Sparse Core Ops, SparseCore 0:
  9.8 55.1 all-gather.4
  66.8 76.1 all-gather.10
  144.8 52.5 all-gather.6
  199.8 43.8 all-gather.8
where the time goes:
time: 330 us; the launch traced here: 329 us
  waiting for transfers between devices  196 us (59%)
  blocking collectives  80.5 us (24%)
  matrix products  19.2 us (6%)
  between operations  13.8 us (4%)
  local copies, waits for them, and re-layouts  11.4 us (3%)
  starting transfers between devices  7.33 us (2%)
    psum x1, blocking collectives, local(): input_grad = lax.psum(partial_value, 'tp').astype(jnp.bfloat16)  70.7 us
    all_gather x1, waiting for transfers between devices, local(): lax.all_gather(down_weight, 'fs', axis=1, tiled=True)  54.8 us
    all_gather x1, waiting for transfers between devices, local(): lax.all_gather(pre_grad, 'fs', axis=0, tiled=True)  41.9 us
    all_gather x1, waiting for transfers between devices, local(): lax.all_gather(up_weight, 'fs', axis=0, tiled=True)  37.4 us
    all_to_all x1, waiting for transfers between devices, local(): lax.all_to_all(cotangent, 'fs', split_axis=1, concat_axis=0, tiled=True)  34.6 us
    all_to_all x1, waiting for transfers between devices, local(): lax.all_to_all(inputs, 'fs', split_axis=1, concat_axis=0, tiled=True)  25.8 us
    psum x1, blocking collectives, local(): down_norms = lax.psum(jnp.sum(down_grad * down_grad, axis=1), 'fs')  9.78 us
    dot_general x2, matrix products, contract_first(): lax.dot_general(left, right, (((0,), (0,)), ((), ())), preferred_element_...  9.7 us
  transfers between devices with their start and end apart: 6, of which 5 were waited for; matrix products, arithmetic and copies ran while one was open for 7% of the time, Pallas kernels for 0%

commit v1 on v0

--- a/solution.py
+++ b/solution.py
@@ -2,6 +2,12 @@
 import jax.numpy as jnp
 from jax import lax
 from jax.sharding import PartitionSpec as P
+
+
+def summed_here(block, axis):
+    blocks = lax.all_gather(block, axis, axis=0, tiled=False)
+    acc = blocks.sum(axis=0)
+    return acc
 
 
 def contract_last(left, right):
@@ -22,7 +28,7 @@
     sq_grad = contract_last(cotangent, lax.all_gather(down_weight, "fs", axis=1, tiled=True))
     pre_grad = (2.0 * active * sq_grad).astype(jnp.bfloat16)
     partial_value = contract_last(pre_grad, lax.all_gather(up_weight, "fs", axis=0, tiled=True))
-    input_grad = lax.psum(partial_value, "tp").astype(jnp.bfloat16)
+    input_grad = summed_here(partial_value, "tp").astype(jnp.bfloat16)
     input_cols, cotan_cols = (
         lax.all_to_all(inputs, "fs", split_axis=1, concat_axis=0, tiled=True),
         lax.all_to_all(cotangent, "fs", split_axis=1, concat_axis=0, tiled=True),

time: 330 us -> 480 us (1.45)
  waiting for transfers between devices: 196 us -> 389 us
  blocking collectives: 80.5 us -> 27.3 us
  other arithmetic: 1.08 us -> 11.8 us
    all_gather x0 -> x1, waiting for transfers between devices: none -> 198 us  [summed_here(): blocks = lax.all_gather(block, axis, axis=0, tiled=False)]
    psum x1, blocking collectives: 70.7 us -> 17.4 us  [local(): up_norms = lax.psum(jnp.sum(up_grad * up_grad, axis=1), 'tp')]
    all_gather x1, waiting for transfers between devices: 41.9 us -> 28 us  [local(): lax.all_gather(pre_grad, 'fs', axis=0, tiled=True)]
    all_gather x1, waiting for transfers between devices: 37.4 us -> 49.5 us  [local(): lax.all_gather(up_weight, 'fs', axis=0, tiled=True)]
    reduce_sum x0 -> x1, other arithmetic: none -> 10.7 us  [summed_here(): acc = blocks.sum(axis=0)]
  transfers between devices with their start and end apart: 6 -> 7, of which waited for: 5 -> 6; matrix products, arithmetic and copies ran while one was open for 7% -> 6% of each run, Pallas kernels for 0% -> 0%
where the time goes in v1:
time: 480 us
  waiting for transfers between devices  389 us (81%)
  blocking collectives  27.3 us (6%)
  matrix products  19.2 us (4%)
  between operations  13.8 us (3%)
  other arithmetic  11.8 us (2%)
  local copies, waits for them, and re-layouts  11.4 us (2%)
  starting transfers between devices  7.44 us (2%)
    all_gather x1, waiting for transfers between devices, summed_here(): blocks = lax.all_gather(block, axis, axis=0, tiled=False)  198 us
    all_gather x1, waiting for transfers between devices, local(): lax.all_gather(down_weight, 'fs', axis=1, tiled=True)  55.1 us
    all_gather x1, waiting for transfers between devices, local(): lax.all_gather(up_weight, 'fs', axis=0, tiled=True)  49.5 us
    all_to_all x1, waiting for transfers between devices, local(): lax.all_to_all(cotangent, 'fs', split_axis=1, concat_axis=0, tiled=True)  32.9 us
    all_gather x1, waiting for transfers between devices, local(): lax.all_gather(pre_grad, 'fs', axis=0, tiled=True)  28 us
    all_to_all x1, waiting for transfers between devices, local(): lax.all_to_all(inputs, 'fs', split_axis=1, concat_axis=0, tiled=True)  23.9 us
    psum x1, blocking collectives, local(): up_norms = lax.psum(jnp.sum(up_grad * up_grad, axis=1), 'tp')  17.4 us
    dot_general x2, matrix products, contract_last(): lax.dot_general(left, right, (((1,), (1,)), ((), ())), preferred_element_...  10.8 us
  transfers between devices with their start and end apart: 7, of which 6 were waited for; matrix products, arithmetic and copies ran while one was open for 6% of the time, Pallas kernels for 0%

profile of v1, /device:TPU:0, one launch (start us, length us, event | category | flops | bytes accessed | tf_op | source)
XLA Modules:
  0.0 479.8 jit_solution(7824727163421122589)
XLA Ops:
  8.0 0.7 all-gather.9.cloned.1.call-update
  8.7 1.1 multiply_convert_fusion
  9.9 55.1 %all-gather.7.cloned.1.call-done = bf16[1024,2048]{1,0:T(8,128)(2,1)} async-done(((bf16[1024,512]{1,0:T(8,128)(2,1)}), bf16[1024,2048]{1,0:T(8,128)(2,1)}) %all-gather.7.cloned.1.call-update) | async-done | bytes 4194320 | tf_op jit(solution)/shard_map/all_gather | solution.py:28
  65.0 4.9 %multiply_convert_fusion.1 = bf16[384,1024]{1,0:T(8,128)(2,1)} fusion(bf16[384,1024]{1,0:T(8,128)(2,1)S(1)} %copy-done.2, bf16[384,2048]{1,0:T(8,128)(2,1)S(1)} %copy-done.1, bf16[1024,2048]{1,0:T(8,128)(2,1)} %all-gather.7.cloned.1.call-done), kind=kOutput, calls=%fused_computation.4 | convolution fusion | flops 1612578816 | bytes 7340032 | tf_op jit(solution)/shard_map/dot_general | solution.py:14
  70.0 49.5 %all-gather.9.cloned.1.call-done = bf16[2048,1024]{1,0:T(8,128)(2,1)} async-done(((bf16[512,1024]{1,0:T(8,128)(2,1)}), bf16[2048,1024]{1,0:T(8,128)(2,1)}) %all-gather.9.cloned.1.call-update) | async-done | bytes 4194320 | tf_op jit(solution)/shard_map/all_gather | solution.py:30
  119.5 5.9 %fusion = f32[384,2048]{1,0:T(8,128)} fusion(bf16[384,1024]{1,0:T(8,128)(2,1)} %multiply_convert_fusion.1, bf16[2048,1024]{1,0:T(8,128)(2,1)} %all-gather.9.cloned.1.call-done), kind=kOutput, calls=%fused_computation.6 | convolution fusion | flops 1610612736 | bytes 8126464 | tf_op jit(solution)/shard_map/dot_general | solution.py:14
  125.4 1.4 copy-done
  126.7 1.6 copy.14
  128.3 3.6 all-to-all-start
  131.9 1.6 copy.16
  133.4 23.9 %all-to-all-done = bf16[384,4,512]{0,2,1:T(8,128)(2,1)S(1)} async-done(((bf16[384,4,512]{0,2,1:T(8,128)(2,1)}), bf16[384,4,512]{0,2,1:T(8,128)(2,1)S(1)}, u32[]{:S(2)}, u32[]{:S(2)}) %all-to-all-start) | async-done | bytes 1572896 | tf_op jit(solution)/shard_map/all_to_all | solution.py:33
  157.3 3.7 all-to-all-start.1
  161.0 1.6 copy.15
  162.6 32.9 %all-to-all-done.1 = bf16[384,4,512]{0,2,1:T(8,128)(2,1)S(1)} async-done(((bf16[384,4,512]{0,2,1:T(8,128)(2,1)}), bf16[384,4,512]{0,2,1:T(8,128)(2,1)S(1)}, u32[]{:S(2)}, u32[]{:S(2)}) %all-to-all-start.1) | async-done | bytes 1572896 | tf_op jit(solution)/shard_map/all_to_all | solution.py:34
  195.5 1.6 copy.17
  197.1 4.2 multiply_reduce_fusion
  201.3 1.8 copy.19
  203.1 10.0 %psum.15 = f32[1024]{0:T(1024)} all-reduce(f32[1024]{0:T(1024)S(1)} %get-tuple-element.22), channel_id=1, replica_groups=mesh['fs'=4,'tp'=8] {'fs'}, use_global_device_ids=true, to_apply=%region_4.0 | all-reduce | flops 1024 | bytes 8192 | tf_op jit(solution)/shard_map/psum | solution.py:43
  213.1 28.0 %all-gather.11.cloned.1.call-done = bf16[1536,1024]{1,0:T(8,128)(2,1)} async-done(((bf16[384,1024]{1,0:T(8,128)(2,1)}), bf16[1536,1024]{1,0:T(8,128)(2,1)}) %all-gather.11.cloned.1.call-update) | async-done | bytes 3145744 | tf_op jit(solution)/shard_map/all_gather | solution.py:37
  241.1 4.2 multiply_reduce_fusion.1
  245.3 1.8 copy.18
  247.1 17.4 %psum.14 = f32[512]{0:T(512)} all-reduce(f32[512]{0:T(512)S(1)} %get-tuple-element.20), channel_id=1, replica_groups=mesh['fs'=4,'tp'=8] {'tp'}, use_global_device_ids=true, to_apply=%region_2.0 | all-reduce | flops 512 | bytes 4096 | tf_op jit(solution)/shard_map/psum | solution.py:42
  264.5 198.1 %all-gather.15.cloned.1.call-done = f32[3072,2048]{1,0:T(8,128)} async-done(((f32[384,2048]{1,0:T(8,128)}), f32[3072,2048]{1,0:T(8,128)}) %all-gather.15.cloned.1.call-update) | async-done | bytes 25165840 | tf_op jit(solution)/shard_map/all_gather | solution.py:8
  462.6 10.7 %reduce_sum.27 = bf16[384,2048]{1,0:T(8,128)(2,1)} reduce(f32[8,384,2048]{2,1,0:T(8,128)} %bitcast.17, f32[]{:T(128)} %constant.2.clone.1), dimensions={0}, to_apply=%region_0.0 | reduce | flops 5505024 | bytes 26738692 | tf_op jit(solution)/shard_map/reduce_sum | solution.py:9
  (15 shorter events, 0.9 us)
Async XLA Ops:
  7.2 1.6 copy-start.2
  7.2 57.8 %all-gather.7.cloned.1.call-start = ((), (), s32[]{:S(2)}) async-start(), calls=%async_computation.2 | async-start | bytes 5242880 | tf_op jit(solution)/shard_map/all_gather | solution.py:28
  7.9 57.1 %copy-start.1 = (bf16[384,2048]{1,0:T(8,128)(2,1)S(1)}, bf16[384,2048]{1,0:T(8,128)(2,1)}, u32[]{:S(2)}) copy-start(bf16[384,2048]{1,0:T(8,128)(2,1)} %param.7) | copy-start | bytes 4718596
  7.9 111.5 %all-gather.9.cloned.1.call-start = ((), (), s32[]{:S(2)}) async-start(), calls=%async_computation.3 | async-start | bytes 5242880 | tf_op jit(solution)/shard_map/all_gather | solution.py:30
  8.7 188.5 %all-gather.13.cloned.1.call-start = ((), (), s32[]{:S(2)}) async-start(), calls=%async_computation.5 | async-start | bytes 3932160 | tf_op jit(solution)/shard_map/all_gather | solution.py:38
  9.9 231.2 %all-gather.11.cloned.1.call-start = ((), (), s32[]{:S(2)}) async-start(), calls=%async_computation.4 | async-start | bytes 3932160 | tf_op jit(solution)/shard_map/all_gather | solution.py:37
  69.9 392.6 %all-gather.15.cloned.1.call-start = ((), (), s32[]{:S(2)}) async-start(), calls=%async_computation.6 | async-start | bytes 28311552 | tf_op jit(solution)/shard_map/all_gather | solution.py:8
  125.3 1.4 copy-start
  128.3 29.0 %all-to-all-start = ((bf16[384,4,512]{0,2,1:T(8,128)(2,1)}), bf16[384,4,512]{0,2,1:T(8,128)(2,1)S(1)}, u32[]{:S(2)}, u32[]{:S(2)}) async-start(bf16[384,4,512]{0,2,1:T(8,128)(2,1)} %bitcast.1), calls=%async_computation | async-start | bytes 3145728 | tf_op jit(solution)/shard_map/all_to_all | solution.py:33
  157.3 38.2 %all-to-all-start.1 = ((bf16[384,4,512]{0,2,1:T(8,128)(2,1)}), bf16[384,4,512]{0,2,1:T(8,128)(2,1)S(1)}, u32[]{:S(2)}, u32[]{:S(2)}) async-start(bf16[384,4,512]{0,2,1:T(8,128)(2,1)} %bitcast.5), calls=%async_computation.1 | async-start | bytes 3145728 | tf_op jit(solution)/shard_map/all_to_all | solution.py:34
Sparse Core Ops, SparseCore 0:
  9.8 55.1 all-gather.6
  66.8 52.5 all-gather.8
  121.3 74.4 all-gather.12
  198.1 42.9 all-gather.10
  242.6 219.9 all-gather.14
